TPU v7x, 32 devices: a whole 2x2x4 slice. The times are simulated.
32 devices in a mesh: sp: 4 (over z), fs: 4 (over y, x), tp: 2 (over core).
Axes of the slice: x: 2, y: 2, z: 4, core: 2. Of those that a mesh axis runs over, the one named last changes fastest.
Arguments:
- hidden_in: bfloat16 [4, 1024, 2048], P('fs', 'sp', 'tp'), may hold values from -6 to 6
- sb_query_w: bfloat16 [2048, 1024], P('fs', 'tp'), may hold values from -0.21875 to 0.21875
- sb_key_w: bfloat16 [2048, 1024], P('fs', 'tp'), may hold values from -0.21875 to 0.21875
- sb_value_w: bfloat16 [2048, 1024], P('fs', 'tp'), may hold values from -0.125 to 0.125
- sb_offset: float32 [16], P('tp'), may hold values from -16 to -6
- delta_query_w: bfloat16 [2048, 1024], P('fs', 'tp'), may hold values from -0.125 to 0.125
- delta_key_w: bfloat16 [2048, 1024], P('fs', 'tp'), may hold values from -0.125 to 0.125
- delta_value_w: bfloat16 [2048, 1024], P('fs', 'tp'), may hold values from -0.125 to 0.125
- decay_w: bfloat16 [2048, 8], P(None, 'tp'), may hold values from -0.125 to 0.125
- write_w: bfloat16 [2048, 8], P(None, 'tp'), may hold values from -0.125 to 0.125
- write_bias: float32 [8], P('tp'), may hold values from -7 to 1.5
- decay_log_scale: float32 [8], P('tp'), may hold values from -14 to -3
- decay_shift: float32 [4, 8, 1024], P('fs', 'tp', 'sp'), may hold values from -3 to 0
- head_gain: float32 [128], replicated, may hold values from 0.1 to 1.9
- sb_out_w: bfloat16 [1024, 2048], P('tp'), may hold values from -0.125 to 0.125
- delta_out_w: bfloat16 [1024, 2048], P('tp'), may hold values from -0.125 to 0.125
Outputs:
- mixed_out: bfloat16 [4, 1024, 2048], P('fs', ('sp', 'tp'))
All inputs are finite; a program needn't handle non-finite values.
Results may differ from a plain program's by a relative error of at most 0.015.
Values may be sent and summed in bfloat16 or wider, within the bound.
A program may use at most 128 MiB of HBM per device.

v0:
```python
import jax
import jax.numpy as jnp
from jax import lax
from jax.sharding import PartitionSpec as P

SB_DIM = 64
GDN_DIM = 128
BLOCK = 64
EXACT_MATMUL = lax.Precision.HIGHEST
NORM_EPS = 1e-06


def carried_in(value, axis, combine, identity):
    devices, index = (lax.axis_size(axis), lax.axis_index(axis))
    everything = jax.tree.map(
        lambda part, kind: lax.all_gather(part.astype(kind), axis),
        value,
        (jnp.bfloat16, jnp.bfloat16),
    )
    start = jax.tree.map(
        lambda part, zero: jnp.broadcast_to(jnp.asarray(zero, part.dtype), part.shape),
        value,
        identity,
    )

    def lap(k, before):
        reached = k < index
        new = combine(
            before, jax.tree.map(lambda part, own: part[k].astype(own.dtype), everything, value)
        )
        return jax.tree.map(lambda a, b: jnp.where(reached, a, b), new, before)

    return lax.fori_loop(0, devices, lap, start)


def unit_lower_inverse(strict_part):
    order_size = strict_part.shape[-1]
    powered = strict_part
    inverse = jnp.eye(order_size, dtype=strict_part.dtype) - strict_part
    for repeat_number in range(max(1, (order_size - 1).bit_length()) - 1):
        powered = jnp.einsum("...ij,...jk->...ik", powered, powered, precision=EXACT_MATMUL)
        inverse = inverse + jnp.einsum(
            "...ij,...jk->...ik", inverse, powered, precision=EXACT_MATMUL
        )
    return inverse


def to_blocks(row_data, block_span):
    blocks_count = row_data.shape[0] // block_span
    shaped = row_data.reshape((blocks_count, block_span) + row_data.shape[1:])
    return jnp.swapaxes(shaped, 1, 2)


def from_blocks(blocked):
    swapped = jnp.swapaxes(blocked, 1, 2)
    return swapped.reshape((-1,) + swapped.shape[2:])


def unit_rows(vectors):
    return vectors * lax.rsqrt(jnp.sum(vectors * vectors, axis=-1, keepdims=True) + NORM_EPS)


def delta_inputs(
    query_proj,
    key_proj,
    value_proj,
    decay_pre,
    write_pre,
    write_bias,
    decay_log_scale,
    shift_rows,
    head_count,
    head_size,
):
    query_act = jax.nn.silu(query_proj.astype(jnp.float32)).reshape(-1, head_count, head_size)
    key_act = jax.nn.silu(key_proj.astype(jnp.float32)).reshape(-1, head_count, head_size)
    value_rows = jax.nn.silu(value_proj.astype(jnp.float32)).reshape(-1, head_count, head_size)
    queries = unit_rows(query_act) * head_size ** (-0.5)
    key_rows = unit_rows(key_act)
    log_decay = -jnp.exp(decay_log_scale) * jax.nn.softplus(decay_pre) + shift_rows
    strength = jax.nn.sigmoid(write_pre + write_bias)
    return (queries, key_rows, value_rows, log_decay, strength)


def delta_prepare(queries, key_rows, value_rows, log_decay, strength):
    block_span = queries.shape[2]
    cumulative = jnp.cumsum(log_decay, axis=-1)
    row_place = lax.broadcasted_iota(jnp.int32, (block_span, block_span), 0)
    col_place = lax.broadcasted_iota(jnp.int32, (block_span, block_span), 1)
    inclusive = col_place <= row_place
    strictly = col_place < row_place
    spread = cumulative[..., :, None] - cumulative[..., None, :]
    decay_table = jnp.where(inclusive, jnp.exp(jnp.where(inclusive, spread, 0.0)), 0.0)
    keys_beta = key_rows * strength[..., None]
    lower_part = jnp.where(
        strictly,
        jnp.einsum("nhik,nhjk->nhij", keys_beta, key_rows, precision=EXACT_MATMUL) * decay_table,
        0.0,
    )
    inverse = unit_lower_inverse(lower_part)
    growth = jnp.exp(cumulative)
    state_updates = jnp.einsum(
        "nhij,nhjv->nhiv", inverse, value_rows * strength[..., None], precision=EXACT_MATMUL
    )
    erase_term = jnp.einsum(
        "nhij,nhjk->nhik", inverse, keys_beta * growth[..., None], precision=EXACT_MATMUL
    )
    inside_block = (
        jnp.einsum("nhik,nhjk->nhij", queries, key_rows, precision=EXACT_MATMUL) * decay_table
    )
    boosted_query = queries * growth[..., None]
    damped_keys = key_rows * jnp.exp(cumulative[..., -1:] - cumulative)[..., None]
    decay_per_block = jnp.exp(cumulative[..., -1])
    return (state_updates, erase_term, inside_block, boosted_query, damped_keys, decay_per_block)


def delta_step(memory_state, inputs):
    state_updates, erase_term, inside_block, boosted_query, damped_keys, decay_per_block = inputs
    fixed_values = state_updates - jnp.einsum(
        "mzq,mqc->mzc", erase_term, memory_state, precision=EXACT_MATMUL
    )
    produced_rows = jnp.einsum(
        "mzq,mqc->mzc", boosted_query, memory_state, precision=EXACT_MATMUL
    ) + jnp.einsum("efq,eqn->efn", inside_block, fixed_values, precision=EXACT_MATMUL)
    memory_state = memory_state * decay_per_block[:, None, None] + jnp.einsum(
        "wam,waz->wmz", damped_keys, fixed_values, precision=EXACT_MATMUL
    )
    return (memory_state, produced_rows)


def transition_step(carried, inputs):
    memory_state, transfer = carried
    state_updates, erase_term, inside_block, boosted_query, damped_keys, decay_per_block = inputs
    fixed_values = state_updates - jnp.einsum(
        "mzq,mqc->mzc", erase_term, memory_state, precision=EXACT_MATMUL
    )
    coupling = jnp.einsum("hik,hil->hkl", damped_keys, erase_term, precision=EXACT_MATMUL)
    memory_state = memory_state * decay_per_block[:, None, None] + jnp.einsum(
        "wam,waz->wmz", damped_keys, fixed_values, precision=EXACT_MATMUL
    )
    transfer = transfer * decay_per_block[:, None, None] - jnp.einsum(
        "hkl,hlm->hkm", coupling, transfer, precision=EXACT_MATMUL
    )
    return ((memory_state, transfer), None)


def compose(prior_blocks, following_blocks):
    joined_map = jnp.einsum(
        "hkl,hlm->hkm", following_blocks[0], prior_blocks[0], precision=EXACT_MATMUL
    )
    joined_state = (
        jnp.einsum("djo,dog->djg", following_blocks[0], prior_blocks[1], precision=EXACT_MATMUL)
        + following_blocks[1]
    )
    return (joined_map, joined_state)


def stick_block(queries, key_rows, value_rows, query_place, key_place, offsets):
    scale_factor = queries.shape[-1] ** (-0.5)
    scores = (
        jnp.einsum("qhd,khd->hqk", queries, key_rows, preferred_element_type=jnp.float32)
        * scale_factor
        + offsets[:, None, None]
    )
    visible = key_place[None, :] < query_place[:, None]
    skipped = jnp.where(visible, jax.nn.log_sigmoid(-scores), 0.0)
    beyond = lax.cumsum(skipped, axis=2, reverse=True) - skipped
    weights = jnp.where(visible, jnp.exp(jax.nn.log_sigmoid(scores) + beyond), 0.0).astype(
        jnp.bfloat16
    )
    partial_value = jnp.einsum(
        "hqk,khd->qhd", weights, value_rows, preferred_element_type=jnp.float32
    )
    return (partial_value, jnp.sum(skipped, axis=2).T)


def stick_combine(partials, totals):
    beyond = jnp.cumsum(totals[::-1], axis=0)[::-1] - totals
    return jnp.sum(partials * jnp.exp(beyond)[..., None], axis=0)


def on_device(
    hidden_in,
    sb_query_w,
    sb_key_w,
    sb_value_w,
    sb_offset,
    delta_query_w,
    delta_key_w,
    delta_value_w,
    decay_w,
    write_w,
    write_bias,
    decay_log_scale,
    decay_shift,
    head_gain,
    sb_out_w,
    delta_out_w,
):
    token_rows = hidden_in.shape[1]
    local_in = hidden_in.reshape(token_rows, hidden_in.shape[2])
    gathered = (
        lax.all_gather(sb_query_w, "fs", axis=0, tiled=True),
        lax.all_gather(sb_key_w, "fs", axis=0, tiled=True),
        lax.all_gather(sb_value_w, "fs", axis=0, tiled=True),
        lax.all_gather(delta_query_w, "fs", axis=0, tiled=True),
        lax.all_gather(delta_key_w, "fs", axis=0, tiled=True),
        lax.all_gather(delta_value_w, "fs", axis=0, tiled=True),
    )
    in_weights = tuple(gathered) + (decay_w, write_w)
    portion = lax.all_gather(local_in, "tp", axis=1, tiled=True)
    projected = tuple(
        (jnp.dot(portion, weight, preferred_element_type=jnp.float32) for weight in in_weights)
    )
    sb_heads = sb_offset.shape[0]
    delta_heads = decay_log_scale.shape[0]
    sb_query = projected[0].astype(jnp.bfloat16).reshape(token_rows, sb_heads, SB_DIM)
    sb_keys = projected[1].astype(jnp.bfloat16)
    sb_values = projected[2].astype(jnp.bfloat16)
    shift_rows = decay_shift.reshape(delta_heads, token_rows).T
    queries, key_rows, value_rows, log_decay, strength = delta_inputs(
        projected[3].astype(jnp.bfloat16),
        projected[4].astype(jnp.bfloat16),
        projected[5].astype(jnp.bfloat16),
        projected[6],
        projected[7],
        write_bias,
        decay_log_scale,
        shift_rows,
        delta_heads,
        GDN_DIM,
    )
    prepared = delta_prepare(
        to_blocks(queries, BLOCK),
        to_blocks(key_rows, BLOCK),
        to_blocks(value_rows, BLOCK),
        to_blocks(log_decay, BLOCK),
        to_blocks(strength, BLOCK),
    )
    identity_map = jnp.broadcast_to(
        jnp.eye(GDN_DIM, dtype=jnp.float32), (delta_heads, GDN_DIM, GDN_DIM)
    )
    empty_state = jnp.zeros((delta_heads, GDN_DIM, GDN_DIM), jnp.float32)
    (local_end, local_map), unused_out = lax.scan(
        transition_step, (empty_state, identity_map), prepared
    )
    own_first = lax.axis_index("sp") * token_rows
    query_place = own_first + lax.iota(jnp.int32, token_rows)
    sp_count = lax.axis_size("sp")
    slot_out = jnp.zeros((sp_count, token_rows, sb_heads, SB_DIM), jnp.float32)
    slot_total = jnp.zeros((sp_count, token_rows, sb_heads), jnp.float32)

    def absorb(slot_arrays, address_portion, value_part, shard_first):

        def active(current):
            partial_value, totals = stick_block(
                sb_query,
                address_portion.reshape(token_rows, sb_heads, SB_DIM),
                value_part.reshape(token_rows, sb_heads, SB_DIM),
                query_place,
                shard_first + lax.iota(jnp.int32, token_rows),
                sb_offset,
            )
            slot_index = shard_first // token_rows
            return (
                lax.dynamic_update_index_in_dim(current[0], partial_value, slot_index, 0),
                lax.dynamic_update_index_in_dim(current[1], totals, slot_index, 0),
            )

        def inactive(current):
            return current

        usable = jnp.logical_and(shard_first >= 0, shard_first <= own_first)
        return lax.cond(usable, active, inactive, slot_arrays)

    key_block = lax.all_gather(sb_keys, "sp", axis=0, tiled=True)
    value_block = lax.all_gather(sb_values, "sp", axis=0, tiled=True)

    def per_shard(shard_number, current):
        row_begin = shard_number * token_rows
        return absorb(
            current,
            lax.dynamic_slice_in_dim(key_block, row_begin, token_rows, 0),
            lax.dynamic_slice_in_dim(value_block, row_begin, token_rows, 0),
            row_begin,
        )

    slot_arrays = lax.fori_loop(
        0, key_block.shape[0] // token_rows, per_shard, (slot_out, slot_total)
    )
    unused_map, incoming = carried_in(
        (local_map, local_end), "sp", compose, (identity_map, empty_state)
    )
    sb_mixed = (
        stick_combine(slot_arrays[0], slot_arrays[1])
        .astype(jnp.bfloat16)
        .reshape(token_rows, sb_heads * SB_DIM)
    )
    unused_end, produced_rows = lax.scan(delta_step, incoming, prepared)
    produced_rows = from_blocks(produced_rows)
    normed = (
        produced_rows
        * lax.rsqrt(jnp.mean(produced_rows * produced_rows, axis=-1, keepdims=True) + NORM_EPS)
        * head_gain
    )
    delta_mixed = normed.astype(jnp.bfloat16).reshape(token_rows, delta_heads * GDN_DIM)
    result = lax.psum_scatter(
        (
            jnp.dot(sb_mixed, sb_out_w, preferred_element_type=jnp.float32)
            + jnp.dot(delta_mixed, delta_out_w, preferred_element_type=jnp.float32)
        ).astype(jnp.bfloat16),
        "tp",
        scatter_dimension=0,
        tiled=True,
    ).astype(jnp.float32)
    return result.astype(jnp.bfloat16).reshape(1, result.shape[0], result.shape[1])


def solution(mesh):
    return jax.shard_map(
        on_device,
        mesh=mesh,
        in_specs=(
            P("fs", "sp", "tp"),
            P("fs", "tp"),
            P("fs", "tp"),
            P("fs", "tp"),
            P("tp"),
            P("fs", "tp"),
            P("fs", "tp"),
            P("fs", "tp"),
            P(None, "tp"),
            P(None, "tp"),
            P("tp"),
            P("tp"),
            P("fs", "tp", "sp"),
            P(),
            P("tp", None),
            P("tp", None),
        ),
        out_specs=P("fs", ("sp", "tp"), None),
        check_vma=False,
    )
```

profile of v0, /device:TPU:0, one launch (start us, length us, event | category | flops | bytes accessed | tf_op | source)
XLA Modules:
  0.0 387.4 jit_solution(17021583337816945138)
XLA Ops:
  12.1 8.6 %all-gather.29.cloned.1.call-done = bf16[1,256,2048]{2,1,0:T(8,128)(2,1)} async-done(((bf16[1,256,1024]{2,1,0:T(8,128)(2,1)}), bf16[1,256,2048]{2,1,0:T(8,128)(2,1)}) %all-gather.29.cloned.1.call-update) | async-done | bytes 1048592 | tf_op jit(solution)/shard_map/all_gather | solution.py:211
  20.7 1.6 fusion.111
  23.6 1.6 fusion.67
  25.4 33.6 %all-gather.23.cloned.1.call-done = bf16[2048,512]{1,0:T(8,128)(2,1)} async-done(((bf16[512,512]{1,0:T(8,128)(2,1)}), bf16[2048,512]{1,0:T(8,128)(2,1)}) %all-gather.23.cloned.1.call-update) | async-done | bytes 2097168 | tf_op jit(solution)/shard_map/all_gather | solution.py:207
  58.9 3.7 fusion.116
  65.5 1.3 fusion.60
  71.4 1.4 fusion.124
  72.9 1.4 convolution_add_fusion.6
  74.3 21.7 %all-gather.25.cloned.1.call-done = bf16[2048,512]{1,0:T(8,128)(2,1)} async-done(((bf16[512,512]{1,0:T(8,128)(2,1)}), bf16[2048,512]{1,0:T(8,128)(2,1)}) %all-gather.25.cloned.1.call-update) | async-done | bytes 2097168 | tf_op jit(solution)/shard_map/all_gather | solution.py:208
  96.0 3.5 divide_multiply_fusion.1
  99.5 2.0 reshape_reshape.3
  101.5 1.9 convolution_add_fusion.5
  103.5 2.1 fusion.78
  105.6 1.6 fusion.82
  107.1 25.7 %all-gather.27.cloned.1.call-done = bf16[2048,512]{1,0:T(8,128)(2,1)} async-done(((bf16[512,512]{1,0:T(8,128)(2,1)}), bf16[2048,512]{1,0:T(8,128)(2,1)}) %all-gather.27.cloned.1.call-update) | async-done | bytes 2097168 | tf_op jit(solution)/shard_map/all_gather | solution.py:206
  132.9 3.8 fusion.117
  136.7 2.0 mul.197
  138.7 1.4 reduce_sum.50
  140.3 2.1 reshape.155
  142.3 2.9 bitcast_multiply_fusion.1
  145.3 19.1 %while.57 = (s32[]{:T(128)}, f32[4,128,128]{2,1,0:T(8,128)S(1)}, f32[4,128,128]{2,1,0:T(8,128)S(1)}, f32[4,4]{1,0:T(4,128)S(1)}, f32[4,4,64,128]{3,2,1,0:T(8,128...) while((s32[]{:T(128)}, f32[4,128,128]{2,1,0:T(8,128)S(1)}, ...), condition=%wide.region_12.13_spmd.clone, body=%wide.region_11.12_spmd.clone.sunk | while | flops 252084224 | bytes 3279532 | solution.py:244
  145.3 1.3 convolution_subtract_fusion.7
  146.6 1.5 convolution_add_fusion.14
  148.1 1.5 fusion.213
  151.3 1.5 convolution_add_fusion.14
  152.8 1.5 fusion.213
  156.1 1.5 convolution_add_fusion.14
  157.6 1.5 fusion.213
  160.9 1.5 convolution_add_fusion.14
  162.4 1.5 fusion.213
  165.0 16.0 %all-gather.1 = bf16[16,128,128]{2,1,0:T(8,128)(2,1)} all-gather(bf16[4,128,128]{2,1,0:T(8,128)(2,1)S(1)} %convert_element_type.96), channel_id=3, replica_groups=mesh['sp'=4,'fs'=4,'tp'=2] {'sp'}, dimensions={0}, use_global_device_ids=true | all-gather | bytes 655360 | tf_op jit(solution)/shard_map/all_gather | solution.py:16
  180.9 3.4 convolution_convert_fusion.5
  184.4 17.0 %all-gather.2 = bf16[16,128,128]{2,1,0:T(8,128)(2,1)} all-gather(bf16[4,128,128]{2,1,0:T(8,128)(2,1)S(1)} %convert_element_type.97), channel_id=4, replica_groups=mesh['sp'=4,'fs'=4,'tp'=2] {'sp'}, dimensions={0}, use_global_device_ids=true | all-gather | bytes 655360 | tf_op jit(solution)/shard_map/all_gather | solution.py:16
  201.4 3.0 convolution_multiply_fusion
  204.5 2.2 all-gather.19.cloned.1.call-done
  206.7 3.3 convolution_convert_fusion.3
  210.0 5.3 %while.58 = (s32[]{:T(128)}, f32[4,128,128]{2,1,0:T(8,128)S(1)}, s32[]{:T(128)}, bf16[4,4,128,128]{3,2,1,0:T(8,128)(2,1)}, bf16[4,4,128,128]{3,2,1,0:T(8,128)(2,1)}, /*index=5*/s32[]{:T(128)}, s32[]{:T(128)}) while((s32[]{:T(128)}, f32[4,128,128]{2,1,0:T(8,128)S(1)}, s32[]{:T(128)}, bf16[4,4,128,128]{3,2,1,0:T(8,128)(2,1)}, ...), condition=%wide.region_14.15_spmd.clone, body=%wide.region_13.14_spmd.clone.sunk | while | flops 100990976 | bytes 1575519 | solution.py:33
  210.0 1.3 fusion.216
  214.1 1.3 fusion.216
  215.4 23.9 %while.56 = (s32[]{:T(128)}, f32[4,128,128]{2,1,0:T(8,128)S(1)}, f32[4,4,64,128]{3,2,1,0:T(8,128)S(1)}, f32[4,4]{1,0:T(4,128)}, f32[4,4,64,128]{3,2,1,0:T(8,128)...) while((s32[]{:T(128)}, f32[4,128,128]{2,1,0:T(8,128)S(1)}, ...), condition=%wide.region_17.18_spmd, body=%wide.region_16.17_spmd.sunk | while | flops 176357376 | bytes 2493593 | solution.py:299
  215.5 1.3 convolution_subtract_fusion.6
  217.9 1.3 fusion.203
  219.9 1.5 convolution_add_fusion.13
  221.4 1.3 convolution_subtract_fusion.6
  225.8 1.5 convolution_add_fusion.13
  229.8 1.3 fusion.203
  231.8 1.5 convolution_add_fusion.13
  235.8 1.3 fusion.203
  237.8 1.5 convolution_add_fusion.13
  240.8 2.9 all-gather.17.cloned.1.call-done
  243.7 2.6 convolution_convert_fusion.4
  247.2 26.1 %all-gather.15.cloned.1.call-done = bf16[1024,512]{1,0:T(8,128)(2,1)} async-done(((bf16[256,512]{1,0:T(8,128)(2,1)}), bf16[1024,512]{1,0:T(8,128)(2,1)}) %all-gather.15.cloned.1.call-update) | async-done | bytes 1048592 | tf_op jit(solution)/shard_map/all_gather | solution.py:276
  273.3 2.3 copy.80
  275.6 26.7 %all-gather.21.cloned.1.call-done = bf16[1024,512]{1,0:T(8,128)(2,1)} async-done(((bf16[256,512]{1,0:T(8,128)(2,1)}), bf16[1024,512]{1,0:T(8,128)(2,1)}) %all-gather.21.cloned.1.call-update) | async-done | bytes 1048592 | tf_op jit(solution)/shard_map/all_gather | solution.py:277
  302.3 2.3 copy.81
  304.6 1.6 broadcast_in_dim.81
  306.8 14.7 %while.59 = (s32[]{:T(128)}, f32[4,256,8,64]{1,3,2,0:T(8,128)}, f32[4,256,8]{1,2,0:T(8,128)}, s32[]{:T(128)}, bf16[1024,512]{0,1:T(8,128)(2,1)}, /*index=5*/bf16...) while((s32[]{:T(128)}, f32[4,256,8,64]{1,3,2,0:T(8,128)}, ...), condition=%wide.region_6.7_spmd.clone.clone, body=%wide.region_0.6_spmd.clone.clone.sunk | while | flops 218698256 | bytes 25745960 | solution.py:288
  306.8 14.7 %conditional.4 = ((f32[4,256,8,64]{1,3,2,0:T(8,128)}, f32[4,256,8]{1,2,0:T(8,128)})) conditional(s32[]{:T(128)} %convert_element_type.140, (f32[4,256,8,64]{1,3,2,0:T(8,128)}, f32[4,256,8]{1,2,0:T(8,128)}) %tuple.124, (s32[]{:T(128)}, s32[]{:T(128)}, bf16[1024,512]{0,1:T(8,128)(2,1)}, bf16[256,8,64]{0,2,1:T(8,128)(2,1)}, f32[8]{0:T(128)S(1)}, ...), branch_computations={%region_1.1_spmd, %region_2.0_spmd} | conditional | flops 218698256 | bytes 25744700 | solution.py:274
  308.0 2.7 fusion.17
  310.7 5.1 %fusion.13 = f32[8,256,2,128]{1,0,3,2:T(8,128)S(1)} fusion(f32[8,256,2,128]{1,3,2,0:T(8,128)S(1)} %bitcast.258), kind=kOutput, calls=%fused_computation.18 | output fusion | flops 66584576 | bytes 4194304 | tf_op jit(solution)/shard_map/reduce-window.6
  316.7 3.0 fusion.6
  323.2 1.8 multiply_reduce_fusion
  326.9 1.7 fusion.59
  328.6 51.9 %reduce-scatter.2.cloned.1.call-done = bf16[128,2048]{1,0:T(8,128)(2,1)} async-done(((bf16[256,2048]{1,0:T(8,128)(2,1)}), bf16[128,2048]{1,0:T(8,128)(2,1)}) %reduce-scatter.2.cloned.1.call-update) | async-done | bytes 524304 | tf_op jit(solution)/shard_map/reduce_scatter | solution.py:307
  (152 shorter events, 44.5 us)
Async XLA Ops:
  6.5 318.5 %copy-start = (bf16[512,2048]{1,0:T(8,128)(2,1)S(1)}, bf16[512,2048]{1,0:T(8,128)(2,1)}, u32[]{:S(2)}) copy-start(bf16[512,2048]{1,0:T(8,128)(2,1)} %param.40) | copy-start | bytes 6291460
  6.5 4.9 %copy-start.18 = (f32[4]{0:T(128)S(1)}, f32[4]{0:T(128)}, u32[]{:S(2)}) copy-start(f32[4]{0:T(128)} %param.37) | copy-start | bytes 52
  6.5 4.9 %copy-start.17 = (f32[128]{0:T(128)S(1)}, f32[128]{0:T(128)}, u32[]{:S(2)}) copy-start(f32[128]{0:T(128)} %param.39) | copy-start | bytes 1540
  6.5 14.1 %copy-start.9 = (bf16[2048,4]{0,1:T(4,128)(2,1)S(1)}, bf16[2048,4]{0,1:T(4,128)(2,1)}, u32[]{:S(2)}) copy-start(bf16[2048,4]{0,1:T(4,128)(2,1)} %param.34) | copy-start | bytes 49156
  6.5 14.1 %copy-start.14 = (f32[1,4,256]{2,1,0:T(4,128)S(1)}, f32[1,4,256]{2,1,0:T(4,128)}, u32[]{:S(2)}) copy-start(f32[1,4,256]{2,1,0:T(4,128)} %param.38) | copy-start | bytes 12292
  6.5 14.1 %all-gather.29.cloned.1.call-start = ((), (), s32[]{:S(2)}) async-start(), calls=%async_computation.10 | async-start | bytes 1572864 | tf_op jit(solution)/shard_map/all_gather | solution.py:211
  7.3 16.3 %copy-start.10 = (bf16[2048,4]{0,1:T(4,128)(2,1)S(1)}, bf16[2048,4]{0,1:T(4,128)(2,1)}, u32[]{:S(2)}) copy-start(bf16[2048,4]{0,1:T(4,128)(2,1)} %param.35) | copy-start | bytes 49156
  7.3 16.3 %copy-start.16 = (f32[4]{0:T(128)S(1)}, f32[4]{0:T(128)}, u32[]{:S(2)}) copy-start(f32[4]{0:T(128)} %param.36) | copy-start | bytes 52
  7.3 51.6 %all-gather.23.cloned.1.call-start = ((), (), s32[]{:S(2)}) async-start(), calls=%async_computation.6 | async-start | bytes 2621440 | tf_op jit(solution)/shard_map/all_gather | solution.py:207
  8.1 87.9 %all-gather.25.cloned.1.call-start = ((), (), s32[]{:S(2)}) async-start(), calls=%async_computation.7 | async-start | bytes 2621440 | tf_op jit(solution)/shard_map/all_gather | solution.py:208
  8.8 124.1 %all-gather.27.cloned.1.call-start = ((), (), s32[]{:S(2)}) async-start(), calls=%async_computation.8 | async-start | bytes 2621440 | tf_op jit(solution)/shard_map/all_gather | solution.py:206
  9.4 171.6 %all-gather.13.cloned.1.call-start = ((), (), s32[]{:S(2)}) async-start(), calls=%async_computation.1 | async-start | bytes 2621440 | tf_op jit(solution)/shard_map/all_gather | solution.py:204
  10.0 196.7 %all-gather.19.cloned.1.call-start = ((), (), s32[]{:S(2)}) async-start(), calls=%async_computation.4 | async-start | bytes 2621440 | tf_op jit(solution)/shard_map/all_gather | solution.py:205
  10.5 233.2 %all-gather.17.cloned.1.call-start = ((), (), s32[]{:S(2)}) async-start(), calls=%async_computation.3 | async-start | bytes 2621440 | tf_op jit(solution)/shard_map/all_gather | solution.py:203
  11.3 262.0 %all-gather.15.cloned.1.call-start = ((), (), s32[]{:S(2)}) async-start(), calls=%async_computation.2 | async-start | bytes 1310720 | tf_op jit(solution)/shard_map/all_gather | solution.py:276
  11.3 54.2 %copy-start.13 = (pred[64,64]{1,0:T(8,128)(4,1)}, pred[64,64]{1,0:T(8,128)(4,1)S(1)}, u32[]{:S(2)}) copy-start(pred[64,64]{1,0:T(8,128)(4,1)S(1)} %iota_compare_fusion.1) | copy-start | bytes 12292
  65.5 1.3 copy-start.1
  74.3 27.2 %copy-start.3 = (f32[4,4,64,64]{3,2,1,0:T(8,128)S(1)}, f32[4,4,64,64]{3,2,1,0:T(8,128)}, u32[]{:S(2)}) copy-start(f32[4,4,64,64]{3,2,1,0:T(8,128)} %fusion.124) | copy-start | bytes 786436
  101.5 4.0 %copy-start.5 = (f32[4,64,4,128]{3,2,1,0:T(4,128)S(1)}, f32[4,64,4,128]{3,2,1,0:T(4,128)}, u32[]{:S(2)}) copy-start(f32[4,64,4,128]{3,2,1,0:T(4,128)} %reshape_reshape.3) | copy-start | bytes 1572868
  140.3 5.0 %copy-start.8 = (f32[4,64,4]{1,2,0:T(4,128)}, f32[4,64,4]{1,2,0:T(4,128)S(1)}, u32[]{:S(2)}) copy-start(f32[4,64,4]{1,2,0:T(4,128)S(1)} %copy.89) | copy-start | bytes 12292
  164.4 0.6 copy-start.15
  180.9 20.5 %copy-start.2 = (f32[4,64,4,128]{3,2,1,0:T(4,128)S(1)}, f32[4,64,4,128]{3,2,1,0:T(4,128)}, u32[]{:S(2)}) copy-start(f32[4,64,4,128]{3,2,1,0:T(4,128)} %copy-done.1) | copy-start | bytes 1572868
  184.3 118.0 %all-gather.21.cloned.1.call-start = ((), (), s32[]{:S(2)}) async-start(), calls=%async_computation.5 | async-start | bytes 1310720 | tf_op jit(solution)/shard_map/all_gather | solution.py:277
  210.0 5.4 %copy-start.7 = (f32[4,4,64,128]{3,2,1,0:T(8,128)S(1)}, f32[4,4,64,128]{3,2,1,0:T(8,128)}, u32[]{:S(2)}) copy-start(f32[4,4,64,128]{3,2,1,0:T(8,128)} %custom-call.2) | copy-start | bytes 1572868
  215.4 165.2 %reduce-scatter.2.cloned.1.call-start = ((), (), s32[]{:S(2)}) async-start(), calls=%async_computation.9 | async-start | bytes 1572864 | tf_op jit(solution)/shard_map/reduce_scatter | solution.py:307
  275.6 31.2 %copy-start.11 = (f32[8]{0:T(128)S(1)}, f32[8]{0:T(128)}, u32[]{:S(2)}) copy-start(f32[8]{0:T(128)} %param.30) | copy-start | bytes 100
  325.1 1.1 copy-start.4
  325.1 1.8 copy-start.6
  325.1 1.8 copy-start.12
Sparse Core Ops, SparseCore 0:
  8.9 11.7 all-gather.28
  22.5 36.3 all-gather.22
  60.8 35.1 all-gather.24
  97.7 35.1 all-gather.26
  134.6 35.1 all-gather.12
  171.5 35.1 all-gather.18
  208.5 35.1 all-gather.16
  245.3 27.9 all-gather.14
  274.9 27.3 all-gather.20
  328.7 51.7 reduce-scatter.1
where the time goes:
time: 389 us; the launch traced here: 387 us
  waiting for transfers between devices  204 us (52%)
  matrix products  92.1 us (24%)
  blocking collectives  33 us (8%)
  local copies, waits for them, and re-layouts  26.2 us (7%)
  other arithmetic  17.2 us (4%)
  between operations  14 us (4%)
    reduce_scatter x1, waiting for transfers between devices, on_device(): lax.psum_scatter((jnp.dot(sb_mixed, sb_out_w, preferred_element_type=jnp....  51.9 us
    all_gather x1, waiting for transfers between devices, on_device(): lax.all_gather(delta_key_w, 'fs', axis=0, tiled=True)  33.6 us
    all_gather x2, blocking collectives, carried_in(): lax.all_gather(part.astype(kind), axis)  33 us
    all_gather x1, waiting for transfers between devices, on_device(): value_block = lax.all_gather(sb_values, 'sp', axis=0, tiled=True)  26.7 us
    all_gather x1, waiting for transfers between devices, on_device(): key_block = lax.all_gather(sb_keys, 'sp', axis=0, tiled=True)  26.1 us
    all_gather x1, waiting for transfers between devices, on_device(): lax.all_gather(delta_query_w, 'fs', axis=0, tiled=True)  25.7 us
    dot_general x8, matrix products, on_device(): jnp.dot(portion, weight, preferred_element_type=jnp.float32)  23.6 us
    all_gather x1, waiting for transfers between devices, on_device(): lax.all_gather(delta_value_w, 'fs', axis=0, tiled=True)  21.7 us
  transfers between devices with their start and end apart: 10, of which 9 were waited for; matrix products, arithmetic and copies ran while one was open for 28% of the time, Pallas kernels for 0%

commit v1 on v0

--- a/solution.py
+++ b/solution.py
@@ -273,8 +273,11 @@
         usable = jnp.logical_and(shard_first >= 0, shard_first <= own_first)
         return lax.cond(usable, active, inactive, slot_arrays)
 
-    key_block = lax.all_gather(sb_keys, "sp", axis=0, tiled=True)
-    value_block = lax.all_gather(sb_values, "sp", axis=0, tiled=True)
+    key_block, value_block = jnp.split(
+        lax.all_gather(jnp.concatenate([sb_keys, sb_values], axis=1), "sp", axis=0, tiled=True),
+        [sb_keys.shape[1]],
+        axis=1,
+    )
 
     def per_shard(shard_number, current):
         row_begin = shard_number * token_rows

time: 389 us -> 387 us (level)
  waiting for transfers between devices: 204 us -> 199 us
    all_gather x2 -> x1, waiting for transfers between devices: 52.8 us -> 16.1 us  [on_device(): lax.all_gather(jnp.concatenate([sb_keys, sb_values], axis=1), 'sp', axis=...]
    all_gather x1, waiting for transfers between devices: 0.01 us -> 33.6 us  [on_device(): lax.all_gather(sb_key_w, 'fs', axis=0, tiled=True)]
  transfers between devices with their start and end apart: 10 -> 9, of which waited for: 9 -> 8; matrix products, arithmetic and copies ran while one was open for 28% -> 28% of each run, Pallas kernels for 0% -> 0%
where the time goes in v1:
time: 387 us; the launch traced here: 386 us
  waiting for transfers between devices  199 us (51%)
  matrix products  91.2 us (24%)
  blocking collectives  33.8 us (9%)
  local copies, waits for them, and re-layouts  28 us (7%)
  other arithmetic  18.8 us (5%)
  between operations  13.7 us (4%)
    reduce_scatter x1, waiting for transfers between devices, on_device(): lax.psum_scatter((jnp.dot(sb_mixed, sb_out_w, preferred_element_type=jnp....  51.3 us
    all_gather x2, blocking collectives, carried_in(): lax.all_gather(part.astype(kind), axis)  33.8 us
    all_gather x1, waiting for transfers between devices, on_device(): lax.all_gather(sb_key_w, 'fs', axis=0, tiled=True)  33.6 us
    all_gather x1, waiting for transfers between devices, on_device(): lax.all_gather(delta_key_w, 'fs', axis=0, tiled=True)  33.6 us
    all_gather x1, waiting for transfers between devices, on_device(): lax.all_gather(delta_query_w, 'fs', axis=0, tiled=True)  25.8 us
    dot_general x8, matrix products, on_device(): jnp.dot(portion, weight, preferred_element_type=jnp.float32)  22.9 us
    all_gather x1, waiting for transfers between devices, on_device(): lax.all_gather(delta_value_w, 'fs', axis=0, tiled=True)  21.7 us
    all_gather x1, waiting for transfers between devices, on_device(): lax.all_gather(jnp.concatenate([sb_keys, sb_values], axis=1), 'sp', axis=...  16.1 us
  transfers between devices with their start and end apart: 9, of which 8 were waited for; matrix products, arithmetic and copies ran while one was open for 28% of the time, Pallas kernels for 0%

profile of v1, /device:TPU:0, one launch (start us, length us, event | category | flops | bytes accessed | tf_op | source)
XLA Modules:
  0.0 385.5 jit_solution(8301495533972653030)
XLA Ops:
  12.1 8.6 %all-gather.26.cloned.1.call-done = bf16[1,256,2048]{2,1,0:T(8,128)(2,1)} async-done(((bf16[1,256,1024]{2,1,0:T(8,128)(2,1)}), bf16[1,256,2048]{2,1,0:T(8,128)(2,1)}) %all-gather.26.cloned.1.call-update) | async-done | bytes 1048592 | tf_op jit(solution)/shard_map/all_gather | solution.py:211
  20.7 1.6 fusion.111
  23.6 1.6 fusion.67
  25.4 33.6 %all-gather.20.cloned.1.call-done = bf16[2048,512]{1,0:T(8,128)(2,1)} async-done(((bf16[512,512]{1,0:T(8,128)(2,1)}), bf16[2048,512]{1,0:T(8,128)(2,1)}) %all-gather.20.cloned.1.call-update) | async-done | bytes 2097168 | tf_op jit(solution)/shard_map/all_gather | solution.py:207
  58.9 3.7 fusion.117
  65.5 1.3 fusion.60
  71.4 1.4 fusion.125
  72.8 1.4 convolution_add_fusion.6
  74.3 21.7 %all-gather.22.cloned.1.call-done = bf16[2048,512]{1,0:T(8,128)(2,1)} async-done(((bf16[512,512]{1,0:T(8,128)(2,1)}), bf16[2048,512]{1,0:T(8,128)(2,1)}) %all-gather.22.cloned.1.call-update) | async-done | bytes 2097168 | tf_op jit(solution)/shard_map/all_gather | solution.py:208
  96.0 3.5 divide_multiply_fusion.1
  99.5 2.0 reshape_reshape.3
  101.5 1.9 convolution_add_fusion.5
  103.4 2.1 fusion.78
  105.5 1.6 fusion.82
  107.1 25.8 %all-gather.24.cloned.1.call-done = bf16[2048,512]{1,0:T(8,128)(2,1)} async-done(((bf16[512,512]{1,0:T(8,128)(2,1)}), bf16[2048,512]{1,0:T(8,128)(2,1)}) %all-gather.24.cloned.1.call-update) | async-done | bytes 2097168 | tf_op jit(solution)/shard_map/all_gather | solution.py:206
  132.9 3.8 fusion.118
  136.7 2.0 mul.197
  138.7 1.4 reduce_sum.50
  140.2 2.1 reshape.155
  142.4 2.9 bitcast_multiply_fusion.1
  145.3 19.1 %while.57 = (s32[]{:T(128)}, f32[4,128,128]{2,1,0:T(8,128)S(1)}, f32[4,128,128]{2,1,0:T(8,128)S(1)}, f32[4,4]{1,0:T(4,128)S(1)}, f32[4,4,64,128]{3,2,1,0:T(8,128...) while((s32[]{:T(128)}, f32[4,128,128]{2,1,0:T(8,128)S(1)}, ...), condition=%wide.region_12.13_spmd.clone, body=%wide.region_11.12_spmd.clone.sunk | while | flops 252084224 | bytes 3279532 | solution.py:244
  146.6 1.5 convolution_add_fusion.14
  148.1 1.5 fusion.214
  150.1 1.3 convolution_subtract_fusion.7
  151.4 1.5 convolution_add_fusion.14
  152.9 1.5 fusion.214
  154.9 1.3 convolution_subtract_fusion.7
  156.2 1.5 convolution_add_fusion.14
  157.7 1.5 fusion.214
  160.9 1.5 convolution_add_fusion.14
  162.5 1.5 fusion.214
  165.7 4.1 %all-gather.14.cloned.1.call-done = bf16[2048,512]{1,0:T(8,128)(2,1)} async-done(((bf16[512,512]{1,0:T(8,128)(2,1)}), bf16[2048,512]{1,0:T(8,128)(2,1)}) %all-gather.14.cloned.1.call-update) | async-done | bytes 2097168 | tf_op jit(solution)/shard_map/all_gather | solution.py:205
  169.8 3.3 convolution_convert_fusion.4
  173.1 33.6 %all-gather.12.cloned.1.call-done = bf16[2048,512]{1,0:T(8,128)(2,1)} async-done(((bf16[512,512]{1,0:T(8,128)(2,1)}), bf16[2048,512]{1,0:T(8,128)(2,1)}) %all-gather.12.cloned.1.call-update) | async-done | bytes 2097168 | tf_op jit(solution)/shard_map/all_gather | solution.py:204
  206.7 2.7 convolution_convert_fusion.5
  210.2 16.0 %all-gather.1 = bf16[16,128,128]{2,1,0:T(8,128)(2,1)} all-gather(bf16[4,128,128]{2,1,0:T(8,128)(2,1)S(1)} %convert_element_type.96), channel_id=3, replica_groups=mesh['sp'=4,'fs'=4,'tp'=2] {'sp'}, dimensions={0}, use_global_device_ids=true | all-gather | bytes 655360 | tf_op jit(solution)/shard_map/all_gather | solution.py:16
  226.3 17.7 %all-gather.2 = bf16[16,128,128]{2,1,0:T(8,128)(2,1)} all-gather(bf16[4,128,128]{2,1,0:T(8,128)(2,1)} %convert_element_type.97), channel_id=4, replica_groups=mesh['sp'=4,'fs'=4,'tp'=2] {'sp'}, dimensions={0}, use_global_device_ids=true | all-gather | bytes 655360 | tf_op jit(solution)/shard_map/all_gather | solution.py:16
  244.0 3.0 convolution_multiply_fusion
  247.0 5.3 %while.58 = (s32[]{:T(128)}, f32[4,128,128]{2,1,0:T(8,128)S(1)}, s32[]{:T(128)}, bf16[4,4,128,128]{3,2,1,0:T(8,128)(2,1)}, bf16[4,4,128,128]{3,2,1,0:T(8,128)(2,1)}, /*index=5*/s32[]{:T(128)}, s32[]{:T(128)}) while((s32[]{:T(128)}, f32[4,128,128]{2,1,0:T(8,128)S(1)}, s32[]{:T(128)}, bf16[4,4,128,128]{3,2,1,0:T(8,128)(2,1)}, ...), condition=%wide.region_14.15_spmd.clone, body=%wide.region_13.14_spmd.clone.sunk | while | flops 100990976 | bytes 1575519 | solution.py:33
  247.1 1.3 fusion.217
  252.4 23.9 %while.56 = (s32[]{:T(128)}, f32[4,128,128]{2,1,0:T(8,128)S(1)}, f32[4,4,64,128]{3,2,1,0:T(8,128)S(1)}, f32[4,4]{1,0:T(4,128)}, f32[4,4,64,128]{3,2,1,0:T(8,128)...) while((s32[]{:T(128)}, f32[4,128,128]{2,1,0:T(8,128)S(1)}, ...), condition=%wide.region_17.18_spmd, body=%wide.region_16.17_spmd.sunk | while | flops 176357376 | bytes 2493593 | solution.py:302
  254.9 1.3 fusion.204
  256.9 1.5 convolution_add_fusion.13
  258.4 1.3 convolution_subtract_fusion.6
  260.9 1.3 fusion.204
  262.9 1.5 convolution_add_fusion.13
  266.8 1.3 fusion.204
  268.8 1.5 convolution_add_fusion.13
  272.8 1.3 fusion.204
  274.8 1.5 convolution_add_fusion.13
  277.8 2.6 convolution_convert_fusion.3
  281.3 16.1 %all-gather.16.cloned.1.call-done = bf16[1024,1024]{1,0:T(8,128)(2,1)} async-done(((bf16[256,1024]{1,0:T(8,128)(2,1)}), bf16[1024,1024]{1,0:T(8,128)(2,1)}) %all-gather.16.cloned.1.call-update) | async-done | bytes 2097168 | tf_op jit(solution)/shard_map/all_gather | solution.py:277
  297.4 2.7 fusion.115
  300.1 2.3 copy.80
  302.3 1.3 copy.81
  303.6 1.6 broadcast_in_dim.81
  305.8 14.7 %while.59 = (s32[]{:T(128)}, f32[4,256,8,64]{1,3,2,0:T(8,128)}, f32[4,256,8]{1,2,0:T(8,128)}, s32[]{:T(128)}, bf16[1024,512]{0,1:T(8,128)(2,1)}, /*index=5*/bf16...) while((s32[]{:T(128)}, f32[4,256,8,64]{1,3,2,0:T(8,128)}, ...), condition=%wide.region_6.7_spmd.clone.clone, body=%wide.region_0.6_spmd.clone.clone.sunk | while | flops 218698256 | bytes 25745960 | solution.py:291
  305.8 14.7 %conditional.4 = ((f32[4,256,8,64]{1,3,2,0:T(8,128)}, f32[4,256,8]{1,2,0:T(8,128)})) conditional(s32[]{:T(128)} %convert_element_type.140, (f32[4,256,8,64]{1,3,2,0:T(8,128)}, f32[4,256,8]{1,2,0:T(8,128)}) %tuple.125, (s32[]{:T(128)}, s32[]{:T(128)}, bf16[1024,512]{0,1:T(8,128)(2,1)}, bf16[256,8,64]{0,2,1:T(8,128)(2,1)}, f32[8]{0:T(128)S(1)}, ...), branch_computations={%region_1.1_spmd, %region_2.0_spmd} | conditional | flops 218698256 | bytes 25744700 | solution.py:274
  307.0 2.7 fusion.17
  309.8 5.1 %fusion.13 = f32[8,256,2,128]{1,0,3,2:T(8,128)S(1)} fusion(f32[8,256,2,128]{1,3,2,0:T(8,128)S(1)} %bitcast.258), kind=kOutput, calls=%fused_computation.18 | output fusion | flops 66584576 | bytes 4194304 | tf_op jit(solution)/shard_map/reduce-window.6
  315.7 3.0 fusion.6
  322.3 1.8 multiply_reduce_fusion
  325.9 1.7 fusion.59
  327.7 51.3 %reduce-scatter.2.cloned.1.call-done = bf16[128,2048]{1,0:T(8,128)(2,1)} async-done(((bf16[256,2048]{1,0:T(8,128)(2,1)}), bf16[128,2048]{1,0:T(8,128)(2,1)}) %reduce-scatter.2.cloned.1.call-update) | async-done | bytes 524304 | tf_op jit(solution)/shard_map/reduce_scatter | solution.py:310
  (153 shorter events, 46.0 us)
Async XLA Ops:
  6.5 317.6 %copy-start = (bf16[512,2048]{1,0:T(8,128)(2,1)S(1)}, bf16[512,2048]{1,0:T(8,128)(2,1)}, u32[]{:S(2)}) copy-start(bf16[512,2048]{1,0:T(8,128)(2,1)} %param.40) | copy-start | bytes 6291460
  6.5 4.9 %copy-start.19 = (f32[4]{0:T(128)S(1)}, f32[4]{0:T(128)}, u32[]{:S(2)}) copy-start(f32[4]{0:T(128)} %param.37) | copy-start | bytes 52
  6.5 4.9 %copy-start.18 = (f32[128]{0:T(128)S(1)}, f32[128]{0:T(128)}, u32[]{:S(2)}) copy-start(f32[128]{0:T(128)} %param.39) | copy-start | bytes 1540
  6.5 14.1 %copy-start.10 = (bf16[2048,4]{0,1:T(4,128)(2,1)S(1)}, bf16[2048,4]{0,1:T(4,128)(2,1)}, u32[]{:S(2)}) copy-start(bf16[2048,4]{0,1:T(4,128)(2,1)} %param.34) | copy-start | bytes 49156
  6.5 14.1 %copy-start.15 = (f32[1,4,256]{2,1,0:T(4,128)S(1)}, f32[1,4,256]{2,1,0:T(4,128)}, u32[]{:S(2)}) copy-start(f32[1,4,256]{2,1,0:T(4,128)} %param.38) | copy-start | bytes 12292
  6.5 14.1 %all-gather.26.cloned.1.call-start = ((), (), s32[]{:S(2)}) async-start(), calls=%async_computation.9 | async-start | bytes 1572864 | tf_op jit(solution)/shard_map/all_gather | solution.py:211
  7.3 16.3 %copy-start.11 = (bf16[2048,4]{0,1:T(4,128)(2,1)S(1)}, bf16[2048,4]{0,1:T(4,128)(2,1)}, u32[]{:S(2)}) copy-start(bf16[2048,4]{0,1:T(4,128)(2,1)} %param.35) | copy-start | bytes 49156
  7.3 16.3 %copy-start.17 = (f32[4]{0:T(128)S(1)}, f32[4]{0:T(128)}, u32[]{:S(2)}) copy-start(f32[4]{0:T(128)} %param.36) | copy-start | bytes 52
  7.3 51.6 %all-gather.20.cloned.1.call-start = ((), (), s32[]{:S(2)}) async-start(), calls=%async_computation.5 | async-start | bytes 2621440 | tf_op jit(solution)/shard_map/all_gather | solution.py:207
  8.1 87.9 %all-gather.22.cloned.1.call-start = ((), (), s32[]{:S(2)}) async-start(), calls=%async_computation.6 | async-start | bytes 2621440 | tf_op jit(solution)/shard_map/all_gather | solution.py:208
  8.8 124.1 %all-gather.24.cloned.1.call-start = ((), (), s32[]{:S(2)}) async-start(), calls=%async_computation.7 | async-start | bytes 2621440 | tf_op jit(solution)/shard_map/all_gather | solution.py:206
  9.4 160.4 %all-gather.14.cloned.1.call-start = ((), (), s32[]{:S(2)}) async-start(), calls=%async_computation.2 | async-start | bytes 2621440 | tf_op jit(solution)/shard_map/all_gather | solution.py:205
  10.0 196.8 %all-gather.12.cloned.1.call-start = ((), (), s32[]{:S(2)}) async-start(), calls=%async_computation.1 | async-start | bytes 2621440 | tf_op jit(solution)/shard_map/all_gather | solution.py:204
  10.5 267.3 %all-gather.18.cloned.1.call-start = ((), (), s32[]{:S(2)}) async-start(), calls=%async_computation.4 | async-start | bytes 2621440 | tf_op jit(solution)/shard_map/all_gather | solution.py:203
  11.3 286.1 %all-gather.16.cloned.1.call-start = ((), (), s32[]{:S(2)}) async-start(), calls=%async_computation.3 | async-start | bytes 2621440 | tf_op jit(solution)/shard_map/all_gather | solution.py:277
  11.3 54.2 %copy-start.14 = (pred[64,64]{1,0:T(8,128)(4,1)}, pred[64,64]{1,0:T(8,128)(4,1)S(1)}, u32[]{:S(2)}) copy-start(pred[64,64]{1,0:T(8,128)(4,1)S(1)} %iota_compare_fusion.1) | copy-start | bytes 12292
  65.5 1.3 copy-start.1
  74.3 27.2 %copy-start.3 = (f32[4,4,64,64]{3,2,1,0:T(8,128)S(1)}, f32[4,4,64,64]{3,2,1,0:T(8,128)}, u32[]{:S(2)}) copy-start(f32[4,4,64,64]{3,2,1,0:T(8,128)} %fusion.125) | copy-start | bytes 786436
  101.5 4.0 %copy-start.5 = (f32[4,64,4,128]{3,2,1,0:T(4,128)S(1)}, f32[4,64,4,128]{3,2,1,0:T(4,128)}, u32[]{:S(2)}) copy-start(f32[4,64,4,128]{3,2,1,0:T(4,128)} %reshape_reshape.3) | copy-start | bytes 1572868
  140.2 5.1 %copy-start.9 = (f32[4,64,4]{1,2,0:T(4,128)}, f32[4,64,4]{1,2,0:T(4,128)S(1)}, u32[]{:S(2)}) copy-start(f32[4,64,4]{1,2,0:T(4,128)S(1)} %copy.89) | copy-start | bytes 12292
  164.4 0.6 copy-start.16
  206.7 2.7 copy-start.8
  209.4 34.6 %copy-start.2 = (f32[4,64,4,128]{3,2,1,0:T(4,128)S(1)}, f32[4,64,4,128]{3,2,1,0:T(4,128)}, u32[]{:S(2)}) copy-start(f32[4,64,4,128]{3,2,1,0:T(4,128)} %copy-done.1) | copy-start | bytes 1572868
  247.0 5.4 %copy-start.7 = (f32[4,4,64,128]{3,2,1,0:T(8,128)S(1)}, f32[4,4,64,128]{3,2,1,0:T(8,128)}, u32[]{:S(2)}) copy-start(f32[4,4,64,128]{3,2,1,0:T(8,128)} %custom-call.2) | copy-start | bytes 1572868
  252.4 126.6 %reduce-scatter.2.cloned.1.call-start = ((), (), s32[]{:S(2)}) async-start(), calls=%async_computation.8 | async-start | bytes 1572864 | tf_op jit(solution)/shard_map/reduce_scatter | solution.py:310
  302.3 3.5 copy-start.12
  324.2 1.1 copy-start.4
  324.2 1.8 copy-start.6
  324.2 1.8 copy-start.13
Sparse Core Ops, SparseCore 0:
  8.9 11.7 all-gather.25
  22.5 36.3 all-gather.19
  60.8 35.1 all-gather.21
  97.7 35.1 all-gather.23
  134.6 35.1 all-gather.13
  171.5 35.1 all-gather.11
  208.5 35.1 all-gather.17
  252.5 44.8 all-gather.15
  327.8 51.1 reduce-scatter.1
